TPU v7x, 32 devices: a whole 2x2x4 slice. The times are simulated.
32 devices in a mesh: ep: 8 (over z, x), tp: 4 (over y, core).
Axes of the slice: x: 2, y: 2, z: 4, core: 2. Of those that a mesh axis runs over, the one named last changes fastest.
Arguments:
- tokens_first: bfloat16 [4096, 2048], P('ep'), may hold values from -6 to 6
- attn_gain: float32 [2048], replicated, may hold values from 0.1 to 1.9
- w_query: bfloat16 [2048, 1024], P(None, 'tp'), may hold values from -6 to 6
- key_matrix: bfloat16 [2048, 512], P(None, 'tp'), may hold values from -6 to 6
- value_matrix: bfloat16 [2048, 512], P(None, 'tp'), may hold values from -0.125 to 0.125
- head_sink_logit: float32 [16], P('tp'), may hold values from 1 to 5
- w_output: bfloat16 [1024, 2048], P('tp'), may hold values from -0.75 to 0.75
- tokens_second: bfloat16 [1024, 2048], P('ep'), may hold values from -6 to 6
- ffn_gain: float32 [2048], replicated, may hold values from 0.1 to 1.9
- routes: int32 [1024, 4], P('ep'), may hold values from 0 to 15, all different within a row; in each aligned block of 128 rows (0 to 127, 128 to 255, ...) at most 64 rows name the same one
- route_weight: float32 [1024, 4], P('ep'), may hold values from 0.2 to 1.5
- w_gate_exp: bfloat16 [16, 2048, 2048], P('ep', None, 'tp'), may hold values from -0.125 to 0.125
- w_up_exp: bfloat16 [16, 2048, 2048], P('ep', None, 'tp'), may hold values from -0.125 to 0.125
- w_down_exp: bfloat16 [16, 2048, 2048], P('ep', 'tp'), may hold values from -0.125 to 0.125
- w_gate_shared: bfloat16 [2048, 1024], P(None, 'tp'), may hold values from -0.125 to 0.125
- w_up_shared: bfloat16 [2048, 1024], P(None, 'tp'), may hold values from -0.125 to 0.125
- w_down_shared: bfloat16 [1024, 2048], P('tp'), may hold values from -0.1875 to 0.1875
Outputs:
- mixer_out: bfloat16 [4096, 2048], P(('ep', 'tp'))
- moe_out: bfloat16 [1024, 2048], P('ep', 'tp')
Inputs may be any that keep to these rules, and one draw needn't show every extreme that they name: `routes`: each row names 4 different experts; among the rows of one index of ep no expert is named more than 64 times, a bound that some block reaches.
All inputs are finite; a program needn't handle non-finite values.
Results may differ from a plain program's by a relative error of at most 0.017.
Values may be sent and summed in bfloat16 or wider, within the bound.
A program may use at most 64 MiB of HBM per device.

v0:
```python
import jax
import jax.numpy as jnp
from jax import lax
from jax.sharding import PartitionSpec as P

MODEL_WIDTH = 2048
HEAD_SIZE = 64
BAND_LENGTH = 128


rope_base = 10000.0
norm_eps = 1e-06


def from_behind(value, axis, by):
    devices = lax.axis_size(axis)
    pairs = [(i, i + by) for i in range(devices) if 0 <= i + by < devices]
    return lax.ppermute(value, axis, pairs)


def rms_scale(inputs, gain):
    wide = inputs.astype(jnp.float32)
    scaled = wide * lax.rsqrt(jnp.mean(wide * wide, axis=-1, keepdims=True) + norm_eps)
    return (scaled * gain).astype(jnp.bfloat16)


def apply_rotary(heads, token_positions):
    freqs = rope_base ** (-jnp.arange(0, HEAD_SIZE, 2, dtype=jnp.float32) / HEAD_SIZE)
    angles = token_positions[:, None] * freqs[None, :]
    cosine = jnp.cos(angles)[:, None, :]
    sine = jnp.sin(angles)[:, None, :]
    first_half, second_half = jnp.split(heads, 2, axis=-1)
    return jnp.concatenate(
        [first_half * cosine - second_half * sine, second_half * cosine + first_half * sine],
        axis=-1,
    )


def local(
    tokens_first,
    attn_gain,
    w_query,
    key_matrix,
    value_matrix,
    head_sink_logit,
    w_output,
    tokens_second,
    ffn_gain,
    routes,
    route_weight,
    w_gate_exp,
    w_up_exp,
    w_down_exp,
    w_gate_shared,
    w_up_shared,
    w_down_shared,
):
    rows_first = tokens_first.shape[0]
    norm_input = rms_scale(tokens_first, attn_gain)
    offset = lax.axis_index("ep") * rows_first
    token_positions = (offset + jnp.arange(rows_first, dtype=jnp.int32)).astype(jnp.float32)
    head_count = w_query.shape[1] // HEAD_SIZE
    key_heads = key_matrix.shape[1] // HEAD_SIZE
    head_group = head_count // key_heads
    query_rows = apply_rotary(
        jnp.dot(norm_input, w_query, preferred_element_type=jnp.float32).reshape(
            rows_first, head_count, HEAD_SIZE
        ),
        token_positions,
    ).astype(jnp.bfloat16)
    keys_local = apply_rotary(
        jnp.dot(norm_input, key_matrix, preferred_element_type=jnp.float32).reshape(
            rows_first, key_heads, HEAD_SIZE
        ),
        token_positions,
    ).astype(jnp.bfloat16)
    values_local = (
        jnp.dot(norm_input, value_matrix, preferred_element_type=jnp.float32)
        .astype(jnp.bfloat16)
        .reshape(rows_first, key_heads, HEAD_SIZE)
    )
    keys_before, values_before = from_behind(
        (keys_local[rows_first - BAND_LENGTH :], values_local[rows_first - BAND_LENGTH :]), "ep", 1
    )
    keys_all = jnp.concatenate([keys_before, keys_local], axis=0)
    values_all = jnp.concatenate([values_before, values_local], axis=0)
    layer_block = min(512, rows_first)
    sink_scores = head_sink_logit.reshape(key_heads, head_group)[:, :, None, None]

    def attend(index):
        leading_row = index * layer_block
        block_queries = query_rows.reshape(layer_block, key_heads, head_group, HEAD_SIZE)
        scores = jnp.einsum(
            "qhgd,khd->hgqk", block_queries, keys_all, preferred_element_type=jnp.float32
        ) * HEAD_SIZE ** (-0.5)
        query_pos = offset + leading_row + jnp.arange(layer_block, dtype=jnp.int32)
        key_pos = (
            offset
            + leading_row
            - BAND_LENGTH
            + jnp.arange(layer_block + BAND_LENGTH, dtype=jnp.int32)
        )
        offsets = query_pos[:, None] - key_pos[None, :]
        visible = (offsets >= 0) & (offsets < BAND_LENGTH) & (key_pos[None, :] >= 0)
        scores = jnp.where(visible[None, None], scores, -jnp.inf)
        peak = jnp.maximum(jnp.max(scores, axis=-1, keepdims=True), sink_scores)
        expo = jnp.exp(scores - peak)
        total = jnp.sum(expo, axis=-1, keepdims=True) + jnp.exp(sink_scores - peak)
        weights = (expo / total).astype(jnp.bfloat16)
        mixed = jnp.einsum(
            "hgqk,khd->qhgd", weights, values_all, preferred_element_type=jnp.float32
        )
        return mixed.astype(jnp.bfloat16).reshape(layer_block, head_count * HEAD_SIZE)

    attended = lax.map(attend, jnp.arange(rows_first // layer_block, dtype=jnp.int32)).reshape(
        rows_first, head_count * HEAD_SIZE
    )
    mixer_out = lax.psum_scatter(
        jnp.dot(attended, w_output, preferred_element_type=jnp.float32).astype(jnp.bfloat16),
        "tp",
        scatter_dimension=0,
        tiled=True,
    )
    rows_second = tokens_second.shape[0]
    topk = routes.shape[1]
    exp_dev = w_gate_exp.shape[0]
    n_expdev = lax.axis_size("ep")
    experts = exp_dev * n_expdev
    capacity = max(2, 2 * rows_second * topk // experts)
    slot_count = experts * capacity
    normed_second = rms_scale(tokens_second, ffn_gain)
    flat = routes.reshape(-1)
    onehot = (flat[:, None] == jnp.arange(experts, dtype=jnp.int32)[None, :]).astype(jnp.int32)
    ranks = jnp.sum((jnp.cumsum(onehot, axis=0) - onehot) * onehot, axis=1)
    slots = flat * capacity + ranks
    match = (jnp.arange(slot_count, dtype=jnp.int32)[:, None] == slots[None, :]).reshape(
        slot_count, rows_second, topk
    )
    dispatch = jnp.sum(match.astype(jnp.float32), axis=2).astype(jnp.bfloat16)
    combine = jnp.sum(match.astype(jnp.float32) * route_weight[None, :, :], axis=2)
    width = normed_second.shape[1] // lax.axis_size("tp")
    feature_slice = lax.dynamic_slice_in_dim(normed_second, lax.axis_index("tp") * width, width, 1)
    outgoing = jnp.dot(dispatch, feature_slice, preferred_element_type=jnp.float32).astype(
        jnp.bfloat16
    )
    arrived = lax.all_to_all(outgoing, "ep", split_axis=0, concat_axis=0, tiled=True)
    piece = lax.all_gather(arrived, "tp", axis=1, tiled=True)
    cols = piece.shape[1]
    part = piece.reshape(n_expdev, exp_dev, capacity, cols)
    gate_pre = jnp.einsum("sjcd,jdf->sjcf", part, w_gate_exp, preferred_element_type=jnp.float32)
    up_pre = jnp.einsum("sjcd,jdf->sjcf", part, w_up_exp, preferred_element_type=jnp.float32)
    hidden = (jax.nn.silu(gate_pre) * up_pre).astype(jnp.bfloat16)
    shared_hidden = (
        jax.nn.silu(jnp.dot(normed_second, w_gate_shared, preferred_element_type=jnp.float32))
        * jnp.dot(normed_second, w_up_shared, preferred_element_type=jnp.float32)
    ).astype(jnp.bfloat16)
    routed_term = jnp.einsum(
        "sjcf,jfd->dsjc", hidden, w_down_exp, preferred_element_type=jnp.float32
    ).reshape(lax.axis_size("tp") * (MODEL_WIDTH // lax.axis_size("tp")), slot_count)
    shared_term = lax.dot_general(
        w_down_shared, shared_hidden, (((0,), (1,)), ((), ())), preferred_element_type=jnp.float32
    )
    summed = lax.psum_scatter(
        jnp.concatenate([routed_term, shared_term], axis=1).astype(jnp.bfloat16),
        "tp",
        scatter_dimension=0,
        tiled=True,
    ).astype(jnp.float32)
    routed_part = summed[:, :slot_count].astype(jnp.bfloat16)
    returned = lax.all_to_all(routed_part, "ep", split_axis=1, concat_axis=1, tiled=True)
    weighted = lax.dot_general(
        combine,
        returned.astype(jnp.float32),
        (((0,), (1,)), ((), ())),
        precision=lax.Precision.HIGHEST,
    )
    moe_out = (weighted + summed[:, slot_count:].T).astype(jnp.bfloat16)
    return (mixer_out, moe_out)


def solution(mesh):
    in_specs = (
        P("ep", None),
        P(),
        P(None, "tp"),
        P(None, "tp"),
        P(None, "tp"),
        P("tp"),
        P("tp", None),
        P("ep", None),
        P(),
        P("ep", None),
        P("ep", None),
        P("ep", None, "tp"),
        P("ep", None, "tp"),
        P("ep", "tp", None),
        P(None, "tp"),
        P(None, "tp"),
        P("tp", None),
    )
    out_specs = (P(("ep", "tp"), None), P("ep", "tp"))
    return jax.shard_map(local, mesh=mesh, in_specs=in_specs, out_specs=out_specs, check_vma=False)
```

profile of v0, /device:TPU:0, one launch (start us, length us, event | category | flops | bytes accessed | tf_op | source)
XLA Modules:
  0.0 194.5 jit_solution(10042323882435477261)
XLA Ops:
  7.2 0.9 copy.42
  8.4 1.2 reduce-window.6
  9.5 0.2 slice_reduce_fusion
  10.1 0.7 multiply_add_fusion
  10.8 1.2 fusion.34
  12.0 1.2 convert_reduce_fusion
  13.2 1.2 fusion.36
  14.4 0.4 convolution_convert_fusion.2
  14.9 32.9 %all_to_all.24 = bf16[8,128,512]{2,1,0:T(8,128)(2,1)} all-to-all(bf16[8,128,512]{2,1,0:T(8,128)(2,1)S(1)} %bitcast.121), channel_id=1, replica_groups=mesh['ep'=8,'tp'=4] {'ep'}, dimensions={0} | all-to-all | bytes 2097152 | tf_op jit(solution)/shard_map/all_to_all | solution.py:146
  47.9 0.3 fusion.73
  48.2 2.3 %fusion.16 = bf16[2048,128]{0,1:T(8,128)(2,1)S(1)} fusion(bf16[256,2048]{1,0:T(8,128)(2,1)} %param.33, bf16[128,2048]{1,0:T(8,128)(2,1)S(1)} %fusion.36, bf16[2048,256]{1,0:T(8,128)(2,1)} %param.32, f32[128,256]{1,0:T(8,128)S(1)} %fusion.73), kind=kOutput, calls=%fused_computation.23 | convolution fusion | flops 268894208 | bytes 3276800 | tf_op jit(solution)/shard_map/dot_general | solution.py:160
  50.5 30.9 %all-gather.2.cloned.1.call-done = bf16[1024,2048]{1,0:T(8,128)(2,1)} async-done(((bf16[1024,512]{1,0:T(8,128)(2,1)}), bf16[1024,2048]{1,0:T(8,128)(2,1)}) %all-gather.2.cloned.1.call-update) | async-done | bytes 4194320 | tf_op jit(solution)/shard_map/all_gather | solution.py:147
  81.5 7.2 %fusion.8 = f32[2,8,64,512]{3,2,1,0:T(8,128)} fusion(bf16[2,2048,512]{2,1,0:T(8,128)(2,1)} %param.28, bf16[8,2,64,2048]{3,2,1,0:T(8,128)(2,1)} %bitcast.130), kind=kOutput, calls=%fused_computation.14 | convolution fusion | flops 2147483648 | bytes 10485760 | tf_op jit(solution)/shard_map/sjcd,jdf->sjcf/dot_general | solution.py:150
  88.7 11.8 %convert_bitcast_fusion = bf16[2048,8,2,64]{0,3,1,2:T(8,128)(2,1)} fusion(bf16[2,512,2048]{2,1,0:T(8,128)(2,1)} %param.30, f32[2,8,64,512]{3,2,1,0:T(8,128)} %fusion.8, bf16[2,2048,512]{2,1,0:T(8,128)(2,1)} %param.29, bf16[8,2,64,2048]{3,2,1,0:T(8,128)(2,1)} %bitcast.131), kind=kOutput, calls=%fused_computation.16 | convolution fusion | flops 4300210176 | bytes 18874368 | tf_op jit(solution)/shard_map/sjcf,jfd->dsjc/dot_general | solution.py:157
  100.5 2.5 %copy.48 = bf16[2048,8,2,64]{0,3,2,1:T(8,128)(2,1)S(1)} copy(bf16[2048,8,2,64]{0,3,1,2:T(8,128)(2,1)} %convert_bitcast_fusion) | data formatting | bytes 8388608 | tf_op jit(solution)/shard_map/sjcf,jfd->dsjc/transpose | solution.py:157
  103.0 2.5 %pad_maximum_fusion = bf16[2048,1152]{0,1:T(8,128)(2,1)} fusion(bf16[2048,128]{0,1:T(8,128)(2,1)S(1)} %fusion.16, bf16[2048,1024]{0,1:T(8,128)(2,1)S(1)} %bitcast.118), kind=kLoop, calls=%fused_computation.5 | loop fusion | flops 9437184 | bytes 9437184 | tf_op jit(solution)/shard_map/concatenate | solution.py:164
  105.6 2.2 %fusion.1 = f32[512]{0:T(512)S(1)} fusion(bf16[512,2048]{1,0:T(8,128)(2,1)} %param.17), kind=kLoop, calls=%fused_computation.7 | loop fusion | flops 3145216 | bytes 2099200 | tf_op jit(solution)/shard_map/reduce_sum | solution.py:23
  107.9 0.3 multiply_cosine_fusion
  108.2 2.6 %fusion.70 = f32[512,128]{0,1:T(8,128)S(1)} fusion(bf16[2048,128]{1,0:T(8,128)(2,1)S(1)} %copy-done.4, bf16[512,2048]{1,0:T(8,128)(2,1)} %param.17, f32[2048]{0:T(1024)S(1)} %copy-done.5, f32[512]{0:T(512)S(1)} %add_rsqrt_fusion), kind=kOutput, calls=%fused_computation.105 | convolution fusion | flops 272629760 | bytes 2893824 | tf_op jit(solution)/shard_map/dot_general | solution.py:72
  110.9 4.0 %collective-permute-start.1 = (bf16[128,2,64]{0,2,1:T(8,128)(2,1)S(1)}, bf16[128,2,64]{0,2,1:T(8,128)(2,1)}, u32[]{:S(2)}, u32[]{:S(2)}) collective-permute-start(bf16[128,2,64]{0,2,1:T(8,128)(2,1)S(1)} %pad_maximum_fusion.1), channel_id=1, source_target_pairs={{0,4},{4,8},{8,12},{12,16},{16,20},{20,24},{24,28},{1,5},{5,9},{9,... | collective-permute-start | bytes 98312 | tf_op jit(solution)/shard_map/ppermute | solution.py:18
  114.8 2.1 %convolution_convert_fusion.3 = bf16[512,128]{0,1:T(8,128)(2,1)S(1)} fusion(bf16[2048,128]{1,0:T(8,128)(2,1)} %param.21, bf16[512,2048]{1,0:T(8,128)(2,1)S(1)} %copy-done.1, f32[2048]{0:T(1024)S(1)} %copy-done.5, f32[512]{0:T(512)S(1)} %add_rsqrt_fusion), kind=kOutput, calls=%fused_computation.43 | convolution fusion | flops 272695296 | bytes 2762752 | tf_op jit(solution)/shard_map/dot_general | solution.py:78
  116.9 3.6 %collective-permute-start = (bf16[128,2,64]{0,2,1:T(8,128)(2,1)S(1)}, bf16[128,2,64]{0,2,1:T(8,128)(2,1)}, u32[]{:S(2)}, u32[]{:S(2)}) collective-permute-start(bf16[128,2,64]{0,2,1:T(8,128)(2,1)S(1)} %bitcast.128), channel_id=1, source_target_pairs={{0,4},{4,8},{8,12},{12,16},{16,20},{20,24},{24,28},{1,5},{5,9},{9,... | collective-permute-start | bytes 98312 | tf_op jit(solution)/shard_map/ppermute | solution.py:18
  120.5 2.5 %fusion.68 = f32[512,256]{0,1:T(8,128)S(1)} fusion(bf16[2048,256]{1,0:T(8,128)(2,1)S(1)} %copy-done.3, bf16[512,2048]{1,0:T(8,128)(2,1)} %param.17, f32[2048]{0:T(1024)S(1)} %copy-done.5, f32[512]{0:T(512)S(1)} %add_rsqrt_fusion), kind=kOutput, calls=%fused_computation.104 | convolution fusion | flops 541065216 | bytes 3680256 | tf_op jit(solution)/shard_map/dot_general | solution.py:66
  123.1 0.4 fusion.30
  123.6 1.8 fusion.10
  125.6 1.1 fusion
  126.8 2.4 %fusion.31 = bf16[2,64,2,512]{3,1,2,0:T(8,128)(2,1)S(1)} fusion(f32[2,640,512,2]{2,1,3,0:T(8,128)S(1)} %get-tuple-element.32, f32[2,2,512]{2,1,0:T(2,128)S(1)} %exponential_add_fusion, f32[2,2,512]{2,1,0:T(2,128)S(1)} %broadcast_maximum_fusion, pred[512,640]{0,1:T(8,128)(4,1)S(1)} %fusion.30, bf16[512,2,64]{0,2,1:T(8,128)(2,1)S(1)} %bitcast.129, ...), kind=kOutput, calls=%fused_computation.41 | convolution fusion | flops 174784512 | bytes 6012928 | tf_op jit(solution)/shard_map/while/body/eval_jaxpr/hgqk,khd->qhgd/dot_general | solution.py:110
  129.2 2.1 %convolution_convert_fusion = bf16[512,2048]{1,0:T(8,128)(2,1)} fusion(bf16[512,256]{0,1:T(8,128)(2,1)S(1)} %bitcast.123, bf16[256,2048]{1,0:T(8,128)(2,1)S(1)} %copy-done), kind=kOutput, calls=%fused_computation.20 | convolution fusion | flops 537919488 | bytes 3407872 | tf_op jit(solution)/shard_map/dot_general | solution.py:119
  131.4 22.1 %reduce-scatter.5.cloned.1.call-done = bf16[512,1152]{0,1:T(8,128)(2,1)} async-done(((bf16[2048,1152]{0,1:T(8,128)(2,1)}), bf16[512,1152]{0,1:T(8,128)(2,1)}) %reduce-scatter.5.cloned.1.call-update) | async-done | bytes 1179664 | tf_op jit(solution)/shard_map/reduce_scatter | solution.py:163
  153.5 1.3 slice.32
  154.8 30.9 %all_to_all.25 = bf16[512,8,128]{0,2,1:T(8,128)(2,1)S(1)} all-to-all(bf16[512,8,128]{0,2,1:T(8,128)(2,1)S(1)} %bitcast.122), channel_id=1, replica_groups=mesh['ep'=8,'tp'=4] {'ep'}, dimensions={1} | all-to-all | bytes 2097152 | tf_op jit(solution)/shard_map/all_to_all | solution.py:170
  185.7 2.3 %fusion.32 = bf16[128,512]{1,0:T(8,128)(2,1)} fusion(f32[1024,128]{1,0:T(8,128)S(1)} %get-tuple-element.17, bf16[512,1024]{0,1:T(8,128)(2,1)S(1)} %bitcast.119, bf16[512,1152]{0,1:T(8,128)(2,1)} %reduce-scatter.5.cloned.1.call-done), kind=kOutput, calls=%fused_computation.44 | convolution fusion | flops 805502976 | bytes 1835008 | tf_op jit(solution)/shard_map/dot_general | solution.py:171
  (45 shorter events, 1.2 us)
Async XLA Ops:
  7.2 122.1 %copy-start = (bf16[256,2048]{1,0:T(8,128)(2,1)S(1)}, bf16[256,2048]{1,0:T(8,128)(2,1)}, u32[]{:S(2)}) copy-start(bf16[256,2048]{1,0:T(8,128)(2,1)} %param.23) | copy-start | bytes 3145732
  7.2 40.7 %copy-start.2 = (bf16[2048,256]{1,0:T(8,128)(2,1)S(1)}, bf16[2048,256]{1,0:T(8,128)(2,1)}, u32[]{:S(2)}) copy-start(bf16[2048,256]{1,0:T(8,128)(2,1)} %param.31) | copy-start | bytes 3145732
  7.2 74.3 %all-gather.2.cloned.1.call-start = ((), (), s32[]{:S(2)}) async-start(), calls=%async_computation.5 | async-start | bytes 5242880 | tf_op jit(solution)/shard_map/all_gather | solution.py:147
  47.8 105.6 %reduce-scatter.5.cloned.1.call-start = ((), (), s32[]{:S(2)}) async-start(), calls=%async_computation.6 | async-start | bytes 5898240 | tf_op jit(solution)/shard_map/reduce_scatter | solution.py:163
  105.5 2.7 %copy-start.4 = (bf16[2048,128]{1,0:T(8,128)(2,1)S(1)}, bf16[2048,128]{1,0:T(8,128)(2,1)}, u32[]{:S(2)}) copy-start(bf16[2048,128]{1,0:T(8,128)(2,1)} %param.20) | copy-start | bytes 1572868
  105.5 2.7 %copy-start.5 = (f32[2048]{0:T(1024)S(1)}, f32[2048]{0:T(1024)}, u32[]{:S(2)}) copy-start(f32[2048]{0:T(1024)} %param.18) | copy-start | bytes 24580
  105.5 82.5 %reduce-scatter.3.cloned.1.call-start = ((), (), s32[]{:S(2)}) async-start(), calls=%async_computation.4 | async-start | bytes 2621440 | tf_op jit(solution)/shard_map/reduce_scatter | solution.py:118
  105.6 9.3 %copy-start.1 = (bf16[512,2048]{1,0:T(8,128)(2,1)S(1)}, bf16[512,2048]{1,0:T(8,128)(2,1)}, u32[]{:S(2)}) copy-start(bf16[512,2048]{1,0:T(8,128)(2,1)} %param.17) | copy-start | bytes 6291460
  108.2 12.3 %copy-start.3 = (bf16[2048,256]{1,0:T(8,128)(2,1)S(1)}, bf16[2048,256]{1,0:T(8,128)(2,1)}, u32[]{:S(2)}) copy-start(bf16[2048,256]{1,0:T(8,128)(2,1)} %param.19) | copy-start | bytes 3145732
  110.9 12.8 %collective-permute-start.1 = (bf16[128,2,64]{0,2,1:T(8,128)(2,1)S(1)}, bf16[128,2,64]{0,2,1:T(8,128)(2,1)}, u32[]{:S(2)}, u32[]{:S(2)}) collective-permute-start(bf16[128,2,64]{0,2,1:T(8,128)(2,1)S(1)} %pad_maximum_fusion.1), channel_id=1, source_target_pairs={{0,4},{4,8},{8,12},{12,16},{16,20},{20,24},{24,28},{1,5},{5,9},{9,... | collective-permute-start | bytes 98312 | tf_op jit(solution)/shard_map/ppermute | solution.py:18
  116.9 6.7 %copy-start.6 = (f32[4]{0:T(128)S(1)}, f32[4]{0:T(128)}, u32[]{:S(2)}) copy-start(f32[4]{0:T(128)} %param.22) | copy-start | bytes 52
  116.9 9.9 %collective-permute-start = (bf16[128,2,64]{0,2,1:T(8,128)(2,1)S(1)}, bf16[128,2,64]{0,2,1:T(8,128)(2,1)}, u32[]{:S(2)}, u32[]{:S(2)}) collective-permute-start(bf16[128,2,64]{0,2,1:T(8,128)(2,1)S(1)} %bitcast.128), channel_id=1, source_target_pairs={{0,4},{4,8},{8,12},{12,16},{16,20},{20,24},{24,28},{1,5},{5,9},{9,... | collective-permute-start | bytes 98312 | tf_op jit(solution)/shard_map/ppermute | solution.py:18
Sparse Core Ops, SparseCore 0:
  48.0 33.4 all-gather.1
  105.6 47.7 reduce-scatter.4
  156.6 31.1 reduce-scatter.2
where the time goes:
time: 195 us
  blocking collectives  63.9 us (33%)
  waiting for transfers between devices  53.1 us (27%)
  matrix products  37.9 us (19%)
  between operations  14 us (7%)
  other arithmetic  12.5 us (6%)
  starting transfers between devices  7.63 us (4%)
  local copies, waits for them, and re-layouts  5.45 us (3%)
    all_to_all x1, blocking collectives, local(): lax.all_to_all(outgoing, 'ep', split_axis=0, concat_axis=0, tiled=True)  32.9 us
    all_gather x1, waiting for transfers between devices, local(): piece = lax.all_gather(arrived, 'tp', axis=1, tiled=True)  30.9 us
    all_to_all x1, blocking collectives, local(): lax.all_to_all(routed_part, 'ep', split_axis=1, concat_axis=1, tiled=True)  30.9 us
    reduce_scatter x1, waiting for transfers between devices, local(): lax.psum_scatter(jnp.concatenate([routed_term, shared_term], axis=1).asty...  22.1 us
    dot_general x1, matrix products, local(): jnp.einsum('sjcf,jfd->dsjc', hidden, w_down_exp, preferred_element_type=j...  11.8 us
    ppermute x2, starting transfers between devices, from_behind(): return lax.ppermute(value, axis, pairs)  7.51 us
    dot_general x1, matrix products, local(): jnp.einsum('sjcd,jdf->sjcf', part, w_gate_exp, preferred_element_type=jnp...  7.19 us
  transfers between devices with their start and end apart: 5, of which 2 were waited for; matrix products, arithmetic and copies ran while one was open for 12% of the time, Pallas kernels for 0%

commit v1 on v0

--- a/solution.py
+++ b/solution.py
@@ -1,6 +1,9 @@
+import functools
 import jax
 import jax.numpy as jnp
 from jax import lax
+from jax.experimental import pallas as pl
+from jax.experimental.pallas import tpu as pltpu
 from jax.sharding import PartitionSpec as P
 
 MODEL_WIDTH = 2048
@@ -34,6 +37,411 @@
         [first_half * cosine - second_half * sine, second_half * cosine + first_half * sine],
         axis=-1,
     )
+
+
+MESH = pl.DeviceIdType.MESH
+
+
+def whereabouts():
+    me, t = lax.axis_index("ep"), lax.axis_index("tp")
+    z, x, y, c = me // 2, me % 2, t // 2, t % 2
+    zs = (z, z + 1 - 2 * (z % 2), (z + 2) % 4, 3 - z)
+    return me, x, y, c, zs
+
+
+def cols(yy, cc, width):
+    return pl.ds(pl.multiple_of((yy * 2 + cc) * width, 128), width)
+
+
+def rows_of(index, count):
+    return pl.ds(pl.multiple_of(index * count, 16), count)
+
+
+def gather_kernel(
+    n_ep, x_ref, meta_ref, halo_ref, out_ref, meta_out, halo_out,
+    zs_, zr_, xs_, xr_, ys_, yr_, cs_, cr_, ms_, mr_, hs_, hr_,
+):
+    me, x, y, c, zs = whereabouts()
+    rows, width = x_ref.shape[0], x_ref.shape[1] // 4
+    z_peer = [{"ep": zd * 2 + x, "tp": y * 2 + c} for zd in zs]
+    x_peer = {"ep": zs[0] * 2 + 1 - x, "tp": y * 2 + c}
+    y_peer = {"ep": me, "tp": (1 - y) * 2 + c}
+    c_peer = {"ep": me, "tp": y * 2 + 1 - c}
+    barrier = pltpu.get_barrier_semaphore()
+    for e in range(1, n_ep):
+        pl.semaphore_signal(
+            barrier, inc=1, device_id={"ep": (me + e) % n_ep, "tp": y * 2 + c}, device_id_type=MESH
+        )
+    for peer in (y_peer, c_peer):
+        pl.semaphore_signal(barrier, inc=1, device_id=peer, device_id_type=MESH)
+    pl.semaphore_wait(barrier, n_ep + 1)
+
+    started = []
+
+    def make(blk, yy, peer, send, recv, own=False):
+        at = out_ref.at[rows_of(blk, rows), cols(yy, c, width)]
+        return pltpu.make_async_remote_copy(
+            src_ref=x_ref.at[:, cols(yy, c, width)] if own else at,
+            dst_ref=at, send_sem=send, recv_sem=recv, device_id=peer, device_id_type=MESH,
+        )
+
+    def go(*a, **k):
+        copy = make(*a, **k)
+        copy.start()
+        started.append(copy)
+
+    for d in (3, 2, 1):
+        go(me, y, z_peer[d], zs_.at[d], zr_.at[d], own=True)
+    go(me, y, x_peer, xs_.at[0], xr_.at[0], own=True)
+    go(me, 1 - y, z_peer[1], zs_.at[0], zr_.at[0], own=True)
+    go(me, 1 - y, x_peer, xs_.at[4], xr_.at[4], own=True)
+
+    def meta_copy(e, to):
+        return pltpu.make_async_remote_copy(
+            src_ref=meta_ref, dst_ref=meta_out.at[to], send_sem=ms_.at[e], recv_sem=mr_.at[e],
+            device_id={"ep": (me + e) % n_ep, "tp": y * 2 + c}, device_id_type=MESH,
+        )
+
+    for e in range(1, n_ep):
+        meta_copy(e, me).start()
+    halo = pltpu.make_async_remote_copy(
+        src_ref=halo_ref, dst_ref=halo_out, send_sem=hs_, recv_sem=hr_,
+        device_id={"ep": (me + 1) % n_ep, "tp": y * 2 + c}, device_id_type=MESH,
+    )
+
+    @pl.when(me < n_ep - 1)
+    def _():
+        halo.start()
+
+    @pl.when(me == 0)
+    def _():
+        halo_out[...] = jnp.zeros_like(halo_out)
+
+    out_ref[rows_of(me, rows), :] = x_ref[...]
+    meta_out[me] = meta_ref[...]
+
+    c_list = []
+
+    def arrived(blk, yy, sem, peer):
+        make(blk, yy, peer, sem, sem).wait_recv()
+
+    def to_core(blk, yy):
+        i = len(c_list)
+        c_list.append((blk, yy))
+        go(blk, yy, c_peer, cs_.at[i], cr_.at[i])
+
+    y_list = []
+
+    def to_y(blk):
+        i = len(y_list)
+        y_list.append(blk)
+        go(blk, y, y_peer, ys_.at[i], yr_.at[i])
+
+    def blk(d, xx):
+        return zs[d] * 2 + xx
+
+    for d in (1, 2, 3):
+        arrived(blk(d, x), y, zr_.at[d], c_peer)
+        go(blk(d, x), y, x_peer, xs_.at[d], xr_.at[d])
+        if d != 1:
+            to_y(blk(d, x))
+        to_core(blk(d, x), y)
+    arrived(blk(0, 1 - x), y, xr_.at[0], c_peer)
+    to_core(blk(0, 1 - x), y)
+    arrived(blk(1, x), 1 - y, zr_.at[0], c_peer)
+    to_core(blk(1, x), 1 - y)
+    arrived(blk(0, 1 - x), 1 - y, xr_.at[4], c_peer)
+    to_core(blk(0, 1 - x), 1 - y)
+    for d in (1, 2, 3):
+        arrived(blk(d, 1 - x), y, xr_.at[d], c_peer)
+        to_y(blk(d, 1 - x))
+        to_core(blk(d, 1 - x), y)
+    for i, b in enumerate(list(y_list)):
+        arrived(b, 1 - y, yr_.at[i], c_peer)
+        to_core(b, 1 - y)
+    for i, (b, yy) in enumerate(c_list):
+        at = out_ref.at[rows_of(b, rows), cols(yy, 1 - c, width)]
+        pltpu.make_async_remote_copy(
+            src_ref=at, dst_ref=at, send_sem=cs_.at[i], recv_sem=cr_.at[i],
+            device_id=c_peer, device_id_type=MESH,
+        ).wait_recv()
+    for e in range(1, n_ep):
+        meta_copy(e, (me + n_ep - e) % n_ep).wait_recv()
+
+    @pl.when(me > 0)
+    def _():
+        halo.wait_recv()
+
+    @pl.when(me < n_ep - 1)
+    def _():
+        halo.wait_send()
+
+    for copy in started:
+        copy.wait_send()
+    for e in range(1, n_ep):
+        meta_copy(e, me).wait_send()
+
+
+def gather(x, meta, halo, n_ep):
+    rows, wide = x.shape
+    dma = pltpu.SemaphoreType.DMA
+    vm = pl.BlockSpec(memory_space=pltpu.VMEM)
+    return pl.pallas_call(
+        functools.partial(gather_kernel, n_ep),
+        out_shape=(
+            jax.ShapeDtypeStruct((n_ep * rows, wide), x.dtype),
+            jax.ShapeDtypeStruct((n_ep,) + meta.shape, meta.dtype),
+            jax.ShapeDtypeStruct(halo.shape, halo.dtype),
+        ),
+        in_specs=[vm] * 3,
+        out_specs=(vm, vm, vm),
+        scratch_shapes=[
+            dma((4,)), dma((4,)), dma((5,)), dma((5,)), dma((5,)), dma((5,)),
+            dma((14,)), dma((14,)), dma((n_ep,)), dma((n_ep,)), dma, dma,
+        ],
+        compiler_params=pltpu.CompilerParams(
+            collective_id=0, has_side_effects=True, vmem_limit_bytes=40 * 1024 * 1024
+        ),
+        name="gather_rows",
+    )(x, meta, halo)
+
+
+def ffn_kernel(
+    cap, x_ref, meta_ref, wg_ref, wu_ref, wd_ref, sg_ref, su_ref, sd_ref, out_ref, xs, ys
+):
+    w_count = ys.shape[1] // cap
+    j = pl.program_id(0)
+    exp_dev = pl.num_programs(0)
+    me = lax.axis_index("ep")
+    n_ep, _, rows = meta_ref.shape
+    topk = meta_ref.shape[1] // 2
+    f32 = jnp.float32
+    before = (
+        lax.broadcasted_iota(jnp.int32, (rows, rows), 0)
+        < lax.broadcasted_iota(jnp.int32, (rows, rows), 1)
+    ).astype(f32).astype(jnp.bfloat16)
+
+    def placed(s, jj, weighted):
+        e = (me * exp_dev + jj).astype(f32)
+        named = meta_ref[s, 0:topk, :] == e
+        hit = jnp.sum(named.astype(f32), axis=0, keepdims=True)
+        rank = jnp.dot(
+            jnp.broadcast_to(hit, (16, rows)).astype(jnp.bfloat16), before,
+            preferred_element_type=f32,
+        )[0:1]
+        slot = lax.broadcasted_iota(jnp.int32, (cap, rows), 0).astype(f32)
+        value = hit
+        if weighted:
+            value = jnp.sum(
+                jnp.where(named, meta_ref[s, topk : 2 * topk, :], 0.0), axis=0, keepdims=True
+            )
+        return jnp.where((slot == rank) & (hit > 0.0), value, 0.0)
+
+    for s in range(n_ep):
+        xs[pl.ds(s * cap, cap), :] = jnp.dot(
+            placed(s, j, False).astype(jnp.bfloat16), x_ref[pl.ds(s * rows, rows), :],
+            preferred_element_type=f32,
+        ).astype(jnp.bfloat16)
+    rows_in = xs[...]
+    gate = jnp.dot(rows_in, wg_ref[0], preferred_element_type=f32)
+    up = jnp.dot(rows_in, wu_ref[0], preferred_element_type=f32)
+    hidden = (gate / (1.0 + jnp.exp(-gate)) * up).astype(jnp.bfloat16)
+    res = jnp.dot(hidden, wd_ref[0], preferred_element_type=f32).astype(jnp.bfloat16)
+    for s in range(n_ep):
+        ys[s, pl.ds(pl.multiple_of(j * cap, cap), cap), :] = res[s * cap : (s + 1) * cap]
+
+    @pl.when(j == exp_dev - 1)
+    def _():
+        for s in range(n_ep):
+            mix = jnp.concatenate([placed(s, jj, True) for jj in range(w_count)], axis=0)
+            out_ref[pl.ds(s * rows, rows), :] = jnp.dot(
+                mix.T.astype(jnp.bfloat16), ys[s], preferred_element_type=f32
+            ).astype(jnp.bfloat16)
+        mine = rows_of(me, rows)
+        own = x_ref[mine, :]
+        sg = jnp.dot(own, sg_ref[...], preferred_element_type=f32)
+        su = jnp.dot(own, su_ref[...], preferred_element_type=f32)
+        sh = (sg / (1.0 + jnp.exp(-sg)) * su).astype(jnp.bfloat16)
+        out_ref[mine, :] = (
+            out_ref[mine, :].astype(f32) + jnp.dot(sh, sd_ref[...], preferred_element_type=f32)
+        ).astype(jnp.bfloat16)
+
+
+def experts_of(x, meta, wg, wu, wd, sg, su, sd, cap):
+    n_ep, _, rows = meta.shape
+    exp_dev, wide, hid = wg.shape
+    vm = pl.BlockSpec(memory_space=pltpu.VMEM)
+    return pl.pallas_call(
+        functools.partial(ffn_kernel, cap),
+        grid=(exp_dev,),
+        out_shape=jax.ShapeDtypeStruct(x.shape, jnp.bfloat16),
+        in_specs=[
+            vm, vm,
+            pl.BlockSpec((1, wide, hid), lambda j: (j, 0, 0)),
+            pl.BlockSpec((1, wide, hid), lambda j: (j, 0, 0)),
+            pl.BlockSpec((1, hid, wide), lambda j: (j, 0, 0)),
+            vm, vm, vm,
+        ],
+        out_specs=vm,
+        scratch_shapes=[
+            pltpu.VMEM((n_ep * cap, wide), jnp.bfloat16),
+            pltpu.VMEM((n_ep, exp_dev * cap, wide), jnp.bfloat16),
+        ],
+        compiler_params=pltpu.CompilerParams(
+            dimension_semantics=("arbitrary",), vmem_limit_bytes=58 * 1024 * 1024
+        ),
+        name="experts",
+    )(x, meta, wg, wu, wd, sg, su, sd)
+
+
+def reduce_kernel(
+    moe_ref, mix_ref, moe_out, mix_out, rc, s1, rx, s2, keep, ry, s3, rz, mrc, ms, mry,
+    cs_, cr_, xs_, xr_, ys_, yr_, zs_, zr_, ms_, mr_,
+):
+    me, x, y, c, zs = whereabouts()
+    rows, width = moe_out.shape
+    mrows = mix_out.shape[0]
+    f32 = jnp.float32
+    x_peer = {"ep": zs[0] * 2 + 1 - x, "tp": y * 2 + c}
+    y_peer = {"ep": me, "tp": (1 - y) * 2 + c}
+    c_peer = {"ep": me, "tp": y * 2 + 1 - c}
+    z_peer = [{"ep": zd * 2 + x, "tp": y * 2 + c} for zd in zs]
+    barrier = pltpu.get_barrier_semaphore()
+    for peer in [x_peer, y_peer, c_peer] + z_peer[1:]:
+        pl.semaphore_signal(barrier, inc=1, device_id=peer, device_id_type=MESH)
+    pl.semaphore_wait(barrier, 6)
+    started = []
+
+    def copy(src, dst, peer, send, recv):
+        return pltpu.make_async_remote_copy(
+            src_ref=src, dst_ref=dst, send_sem=send, recv_sem=recv,
+            device_id=peer, device_id_type=MESH,
+        )
+
+    def go(*a):
+        k = copy(*a)
+        k.start()
+        started.append(k)
+
+    def got(dst, recv):
+        copy(dst, dst, c_peer, recv, recv).wait_recv()
+
+    ysel = (1 - y, y)
+    order = (2, 3, 1, 0)
+
+    def mine(d, xx, yy, cc):
+        return (rows_of(zs[d] * 2 + xx, rows), cols(yy, cc, width))
+
+    def mixer_core(k):
+        go(
+            mix_ref.at[rows_of(ysel[k] * 2 + 1 - c, mrows), :], mrc.at[k], c_peer,
+            ms_.at[k], mr_.at[k],
+        )
+
+    def core(d, col, k):
+        i = d * 4 + col * 2 + k
+        xx = (1 - x, x)[col]
+        at = mine(d, xx, ysel[k], 1 - c)
+        go(moe_ref.at[at[0], at[1]], rc.at[i], c_peer, cs_.at[i], cr_.at[i])
+
+    core(order[0], 0, 0)
+    core(order[0], 0, 1)
+    mixer_core(0)
+    for d in order[1:]:
+        core(d, 0, 0)
+        core(d, 0, 1)
+    for d in order:
+        core(d, 1, 0)
+        core(d, 1, 1)
+    mixer_core(1)
+
+    def pair(d, col, k):
+        i = d * 4 + col * 2 + k
+        xx = (1 - x, x)[col]
+        at = mine(d, xx, ysel[k], c)
+        got(rc.at[i], cr_.at[i])
+        return moe_ref[at[0], at[1]].astype(f32) + rc[i].astype(f32)
+
+    def x_send(d):
+        for k in (0, 1):
+            i = d * 2 + k
+            s1[i] = pair(d, 0, k).astype(jnp.bfloat16)
+            go(s1.at[i], rx.at[i], x_peer, xs_.at[i], xr_.at[i])
+
+    x_send(order[0])
+    got(mrc.at[0], mr_.at[0])
+    ms[...] = (
+        mix_ref[rows_of(ysel[0] * 2 + c, mrows), :].astype(f32) + mrc[0].astype(f32)
+    ).astype(jnp.bfloat16)
+    go(ms, mry, y_peer, ms_.at[2], mr_.at[2])
+    for d in order[1:]:
+        x_send(d)
+    for d in order:
+        for k in (0, 1):
+            i = d * 2 + k
+            part = pair(d, 1, k)
+            got(rx.at[i], xr_.at[i])
+            part = part + rx[i].astype(f32)
+            if k == 0:
+                s2[d] = part.astype(jnp.bfloat16)
+                go(s2.at[d], ry.at[d], y_peer, ys_.at[d], yr_.at[d])
+            else:
+                keep[d] = part
+    for d in order[:3]:
+        got(ry.at[d], yr_.at[d])
+        s3[d] = (keep[d] + ry[d].astype(f32)).astype(jnp.bfloat16)
+        go(s3.at[d], rz.at[d], z_peer[d], zs_.at[d], zr_.at[d])
+    got(mrc.at[1], mr_.at[1])
+    got(mry, mr_.at[2])
+    mix_out[...] = (
+        mix_ref[rows_of(ysel[1] * 2 + c, mrows), :].astype(f32)
+        + mrc[1].astype(f32)
+        + mry[...].astype(f32)
+    ).astype(jnp.bfloat16)
+    got(ry.at[0], yr_.at[0])
+    total = keep[0] + ry[0].astype(f32)
+    for d in order[:3]:
+        got(rz.at[d], zr_.at[d])
+        total = total + rz[d].astype(f32)
+    moe_out[...] = total.astype(jnp.bfloat16)
+    for k in started:
+        k.wait_send()
+
+
+def reduce_both(moe, mix, n_ep):
+    rows, width = moe.shape[0] // n_ep, moe.shape[1] // 4
+    mrows, wide = mix.shape[0] // 4, mix.shape[1]
+    dma = pltpu.SemaphoreType.DMA
+    vm = pl.BlockSpec(memory_space=pltpu.VMEM)
+    bf = jnp.bfloat16
+    return pl.pallas_call(
+        reduce_kernel,
+        out_shape=(
+            jax.ShapeDtypeStruct((rows, width), bf),
+            jax.ShapeDtypeStruct((mrows, wide), bf),
+        ),
+        in_specs=[vm, vm],
+        out_specs=(vm, vm),
+        scratch_shapes=[
+            pltpu.VMEM((16, rows, width), bf),
+            pltpu.VMEM((8, rows, width), bf),
+            pltpu.VMEM((8, rows, width), bf),
+            pltpu.VMEM((4, rows, width), bf),
+            pltpu.VMEM((4, rows, width), jnp.float32),
+            pltpu.VMEM((4, rows, width), bf),
+            pltpu.VMEM((4, rows, width), bf),
+            pltpu.VMEM((4, rows, width), bf),
+            pltpu.VMEM((2, mrows, wide), bf),
+            pltpu.VMEM((mrows, wide), bf),
+            pltpu.VMEM((mrows, wide), bf),
+            dma((16,)), dma((16,)), dma((8,)), dma((8,)), dma((4,)), dma((4,)),
+            dma((4,)), dma((4,)), dma((3,)), dma((3,)),
+        ],
+        compiler_params=pltpu.CompilerParams(
+            collective_id=1, has_side_effects=True, vmem_limit_bytes=40 * 1024 * 1024
+        ),
+        name="reduce_both",
+    )(moe, mix)
 
 
 def local(
@@ -79,9 +487,27 @@
         .astype(jnp.bfloat16)
         .reshape(rows_first, key_heads, HEAD_SIZE)
     )
-    keys_before, values_before = from_behind(
-        (keys_local[rows_first - BAND_LENGTH :], values_local[rows_first - BAND_LENGTH :]), "ep", 1
-    )
+    kernels = lax.axis_size("ep") == 8 and lax.axis_size("tp") == 4
+    if kernels:
+        normed_second = rms_scale(tokens_second, ffn_gain)
+        meta = jnp.concatenate([routes.astype(jnp.float32), route_weight], axis=1).T
+        halo = jnp.concatenate(
+            [
+                keys_local[rows_first - BAND_LENGTH :].reshape(BAND_LENGTH, -1),
+                values_local[rows_first - BAND_LENGTH :].reshape(BAND_LENGTH, -1),
+            ],
+            axis=1,
+        )
+        gathered, metas, before = gather(normed_second, meta, halo, lax.axis_size("ep"))
+        split = key_heads * HEAD_SIZE
+        keys_before = before[:, :split].reshape(BAND_LENGTH, key_heads, HEAD_SIZE)
+        values_before = before[:, split:].reshape(BAND_LENGTH, key_heads, HEAD_SIZE)
+    else:
+        keys_before, values_before = from_behind(
+            (keys_local[rows_first - BAND_LENGTH :], values_local[rows_first - BAND_LENGTH :]),
+            "ep",
+            1,
+        )
     keys_all = jnp.concatenate([keys_before, keys_local], axis=0)
     values_all = jnp.concatenate([values_before, values_local], axis=0)
     layer_block = min(512, rows_first)
@@ -115,6 +541,17 @@
     attended = lax.map(attend, jnp.arange(rows_first // layer_block, dtype=jnp.int32)).reshape(
         rows_first, head_count * HEAD_SIZE
     )
+    if kernels:
+        capacity = max(2, 2 * tokens_second.shape[0] * routes.shape[1] // (w_gate_exp.shape[0] * 8))
+        mixer_part = jnp.dot(attended, w_output, preferred_element_type=jnp.float32).astype(
+            jnp.bfloat16
+        )
+        moe_part = experts_of(
+            gathered, metas, w_gate_exp, w_up_exp, w_down_exp,
+            w_gate_shared, w_up_shared, w_down_shared, capacity,
+        )
+        moe_out, mixer_out = reduce_both(moe_part, mixer_part, lax.axis_size("ep"))
+        return (mixer_out, moe_out)
     mixer_out = lax.psum_scatter(
         jnp.dot(attended, w_output, preferred_element_type=jnp.float32).astype(jnp.bfloat16),
         "tp",

time: 195 us -> 129 us (0.66)
  Pallas kernels: 0 us -> 96.4 us
  blocking collectives: 63.9 us -> 0 us
  waiting for transfers between devices: 53.1 us -> 0 us
  matrix products: 37.9 us -> 14.2 us
  between operations: 14 us -> 0.88 us
  starting transfers between devices: 7.63 us -> 0 us
    pallas_call x0 -> x3, Pallas kernels: none -> 96.4 us  [the longest x1 38.4 us: reduce_both(): pl.pallas_call(reduce_kernel, out_shape=(jax.ShapeDtypeStruct((rows, widt...]
    all_to_all x2 -> x0, blocking collectives: 63.9 us -> none  [the longest x1 32.9 us: local(): lax.all_to_all(outgoing, 'ep', split_axis=0, concat_axis=0, tiled=True)]
    all_gather x1 -> x0, waiting for transfers between devices: 30.9 us -> none  [local(): piece = lax.all_gather(arrived, 'tp', axis=1, tiled=True)]
    dot_general x6 -> x0, matrix products: 24.4 us -> none  [the longest x1 11.8 us: local(): jnp.einsum('sjcf,jfd->dsjc', hidden, w_down_exp, preferred_element_type=j...]
    reduce_scatter x2 -> x0, waiting for transfers between devices: 22.1 us -> none  [the longest x1 22.1 us: local(): lax.psum_scatter(jnp.concatenate([routed_term, shared_term], axis=1).asty...]
    ppermute x2 -> x0, starting transfers between devices: 7.51 us -> none  [from_behind(): return lax.ppermute(value, axis, pairs)]
    unnamed x15 -> x20, local copies, waits for them, and re-layouts: 0.97 us -> 5.46 us
    transpose x1 -> x0, local copies, waits for them, and re-layouts: 2.49 us -> none  [local(): jnp.einsum('sjcf,jfd->dsjc', hidden, w_down_exp, preferred_element_type=j...]
  transfers between devices with their start and end apart: 5 -> 0, of which waited for: 2 -> 0; matrix products, arithmetic and copies ran while one was open for 12% -> 0% of each run, Pallas kernels for 0% -> 0%
where the time goes in v1:
time: 129 us; the launch traced here: 128 us
  Pallas kernels  96.4 us (75%)
  matrix products  14.2 us (11%)
  other arithmetic  10.7 us (8%)
  local copies, waits for them, and re-layouts  6 us (5%)
    pallas_call x1, Pallas kernels, reduce_both(): pl.pallas_call(reduce_kernel, out_shape=(jax.ShapeDtypeStruct((rows, widt...  38.4 us
    pallas_call x1, Pallas kernels, gather(): pl.pallas_call(functools.partial(gather_kernel, n_ep), out_shape=(jax.Sha...  36.6 us
    pallas_call x1, Pallas kernels, experts_of(): pl.pallas_call(functools.partial(ffn_kernel, cap), grid=(exp_dev,), out_s...  21.4 us
    unnamed x20, local copies, waits for them, and re-layouts  5.46 us
    dot_general x1, matrix products, attend(): jnp.einsum('hgqk,khd->qhgd', weights, values_all, preferred_element_type=...  4.14 us
    reduce_sum x1, other arithmetic, attend(): total = jnp.sum(expo, axis=-1, keepdims=True) + jnp.exp(sink_scores - peak)  3.61 us
    reduce_sum x2, other arithmetic, rms_scale(): jnp.mean(wide * wide, axis=-1, keepdims=True) + norm_eps  3.45 us
    dot_general x1, matrix products, attend(): jnp.einsum('qhgd,khd->hgqk', block_queries, keys_all, preferred_element_t...  3.4 us

profile of v1, /device:TPU:0, one launch (start us, length us, event | category | flops | bytes accessed | tf_op | source)
XLA Modules:
  0.0 128.2 jit_solution(14635602546046114264)
XLA Ops:
  0.6 0.0 copy-start
  0.6 0.0 copy-start.4
  0.7 1.4 %fusion.9 = f32[128]{0:T(128)S(1)} fusion(bf16[128,2048]{1,0:T(8,128)(2,1)} %param.24), kind=kLoop, calls=%fused_computation.20 | loop fusion | flops 786304 | bytes 524800 | tf_op jit(solution)/shard_map/reduce_sum | solution.py:26
  2.1 1.2 fusion.11.x_ref
  3.3 0.7 convert_element_type.44
  4.0 0.7 maximum_bitcast_fusion.4.meta_ref
  4.7 2.1 %fusion.1 = f32[512]{0:T(512)S(1)} fusion(bf16[512,2048]{1,0:T(8,128)(2,1)} %param.17), kind=kLoop, calls=%fused_computation.6 | loop fusion | flops 3145216 | bytes 2099200 | tf_op jit(solution)/shard_map/reduce_sum | solution.py:26
  6.8 2.5 %convolution_convert_fusion.1 = bf16[512,128]{1,0:T(8,128)(2,1)S(1)} fusion(bf16[2048,128]{1,0:T(8,128)(2,1)} %param.21, bf16[512,2048]{1,0:T(8,128)(2,1)} %param.17, f32[2048]{0:T(1024)} %param.18, f32[512]{0:T(512)S(1)} %add_rsqrt_fusion), kind=kOutput, calls=%fused_computation.19 | convolution fusion | flops 272695296 | bytes 2762752 | tf_op jit(solution)/shard_map/dot_general | solution.py:486
  9.3 0.9 fusion.30
  10.2 0.3 multiply_cosine_fusion
  10.6 0.1 copy.26
  10.8 36.6 %gather_rows.1 = (bf16[1024,2048]{1,0:T(8,128)(2,1)S(1)}, f32[8,8,128]{2,1,0:T(8,128)S(1)}, bf16[128,256]{1,0:T(8,128)(2,1)S(1)}) custom-call(bf16[128,2048]{1,0:T(8,128)(2,1)S(1)} %fusion.11.x_ref, f32[8,128]{1,0:T(8,128)S(1)} %maximum_bitcast_fusion.4.meta_ref, bf16[128,256]{1,0:T(8,128)(2,1)S(1)} %pad_maximum_fusion.halo_ref), custom_call_target="tpu_custom_call" | custom-call | tf_op jit(solution)/shard_map/gather_rows/pallas_call | solution.py:189
  47.4 1.9 %copy-done.2 = bf16[1024,2048]{1,0:T(8,128)(2,1)} copy-done((bf16[1024,2048]{1,0:T(8,128)(2,1)}, bf16[1024,2048]{1,0:T(8,128)(2,1)S(1)}, u32[]{:S(2)}) %copy-start.2) | copy-done | bytes 4194328
  49.3 0.6 copy-done.3
  49.9 21.4 %experts.1.moe_ref = bf16[1024,2048]{1,0:T(8,128)(2,1)} custom-call(bf16[1024,2048]{1,0:T(8,128)(2,1)} %copy-done.2, f32[8,8,128]{2,1,0:T(8,128)} %copy-done.3, bf16[2,2048,512]{2,1,0:T(8,128)(2,1)} %wg_ref.1, bf16[2,2048,512]{2,1,0:T(8,128)(2,1)} %wu_ref.1, bf16[2,512,2048]{2,1,0:T(8,128)(2,1)} %wd_ref.1, bf16[2048,256]{1,0:T(8,128)(2,1)} %sg_ref.1, ...), custom_call_target="tpu_custom_call" | custom-call | tf_op jit(solution)/shard_map/experts/pallas_call | solution.py:274
  71.3 0.4 fusion.7
  71.7 2.5 %fusion.27 = f32[512,256]{0,1:T(8,128)S(1)} fusion(bf16[2048,256]{1,0:T(8,128)(2,1)S(1)} %copy-done.5, bf16[512,2048]{1,0:T(8,128)(2,1)} %param.17, f32[2048]{0:T(1024)S(1)} %copy-done.7, f32[512]{0:T(512)S(1)} %add_rsqrt_fusion), kind=kOutput, calls=%fused_computation.57 | convolution fusion | flops 541065216 | bytes 3680256 | tf_op jit(solution)/shard_map/dot_general | solution.py:474
  74.3 0.1 subtract_convert_fusion
  74.4 0.1 copy.29
  74.5 3.4 %fusion.4 = (f32[2,2,512]{2,1,0:T(2,128)S(1)}, f32[2,640,512,2]{2,1,3,0:T(8,128)}) fusion(pred[512,640]{0,1:T(8,128)(4,1)S(1)} %fusion.7, bf16[512,2,2,32]{0,3,2,1:T(8,128)(2,1)S(1)} %bitcast.45, bf16[512,2,2,32]{0,3,2,1:T(8,128)(2,1)S(1)} %bitcast.44, bf16[512,2,32]{0,2,1:T(8,128)(2,1)S(1)} %get-tuple-element.36, ...), kind=kOutput, calls=%fused_computation.9 | convolution fusion | flops 172718080 | bytes 6004736 | tf_op jit(solution)/shard_map/while/body/eval_jaxpr/qhgd,khd->hgqk/dot_general | solution.py:519
  77.9 0.1 max.22
  78.0 0.1 broadcast_maximum_fusion
  78.1 3.6 %fusion = f32[2,2,512]{2,1,0:T(2,128)S(1)} fusion(f32[2,640,512,2]{2,1,3,0:T(8,128)} %get-tuple-element.42, f32[2,2,512]{2,1,0:T(2,128)S(1)} %broadcast_maximum_fusion, pred[512,640]{0,1:T(8,128)(4,1)S(1)} %fusion.7), kind=kLoop, calls=%fused_computation.5 | loop fusion | flops 5240832 | bytes 5586944 | tf_op jit(solution)/shard_map/while/body/eval_jaxpr/reduce_sum | solution.py:534
  81.7 0.1 exponential_add_fusion
  81.8 0.1 copy.28
  81.9 0.1 copy.27
  82.0 4.1 %fusion.8 = bf16[2,64,2,512]{3,1,2,0:T(8,128)(2,1)S(1)} fusion(f32[2,640,512,2]{2,1,3,0:T(8,128)} %get-tuple-element.42, f32[2,2,512]{2,1,0:T(2,128)S(1)} %exponential_add_fusion, f32[2,2,512]{2,1,0:T(2,128)S(1)} %broadcast_maximum_fusion, pred[512,640]{0,1:T(8,128)(4,1)S(1)} %fusion.7, bf16[512,2,64]{0,2,1:T(8,128)(2,1)S(1)} %bitcast.47, ...), kind=kOutput, calls=%fused_computation.18 | convolution fusion | flops 174784512 | bytes 6012928 | tf_op jit(solution)/shard_map/while/body/eval_jaxpr/hgqk,khd->qhgd/dot_general | solution.py:536
  86.2 0.7 convolution_convert_fusion.mix_ref
  86.9 1.4 %copy-done.1 = bf16[1024,2048]{1,0:T(8,128)(2,1)S(1)} copy-done((bf16[1024,2048]{1,0:T(8,128)(2,1)S(1)}, bf16[1024,2048]{1,0:T(8,128)(2,1)}, u32[]{:S(2)}) %copy-start.1) | copy-done | bytes 4194328
  88.3 38.4 %reduce_both.1 = (bf16[128,512]{1,0:T(8,128)(2,1)S(1)}, bf16[128,2048]{1,0:T(8,128)(2,1)S(1)}) custom-call(bf16[1024,2048]{1,0:T(8,128)(2,1)S(1)} %copy-done.1, bf16[512,2048]{1,0:T(8,128)(2,1)S(1)} %convolution_convert_fusion.mix_ref), custom_call_target="tpu_custom_call" | custom-call | tf_op jit(solution)/shard_map/reduce_both/pallas_call | solution.py:417
  126.7 0.8 copy.37
  127.5 0.7 copy.38
  (24 shorter events, 0.1 us)
Async XLA Ops:
  0.6 85.5 %copy-start = (bf16[256,2048]{1,0:T(8,128)(2,1)S(1)}, bf16[256,2048]{1,0:T(8,128)(2,1)}, u32[]{:S(2)}) copy-start(bf16[256,2048]{1,0:T(8,128)(2,1)} %param.23) | copy-start | bytes 3145732
  0.6 8.6 %copy-start.4 = (bf16[512,2048]{1,0:T(8,128)(2,1)S(1)}, bf16[512,2048]{1,0:T(8,128)(2,1)}, u32[]{:S(2)}) copy-start(bf16[512,2048]{1,0:T(8,128)(2,1)} %param.17) | copy-start | bytes 6291460
  0.7 8.6 %copy-start.7 = (f32[2048]{0:T(1024)S(1)}, f32[2048]{0:T(1024)}, u32[]{:S(2)}) copy-start(f32[2048]{0:T(1024)} %param.18) | copy-start | bytes 24580
  0.7 8.6 %copy-start.6 = (bf16[2048,128]{1,0:T(8,128)(2,1)S(1)}, bf16[2048,128]{1,0:T(8,128)(2,1)}, u32[]{:S(2)}) copy-start(bf16[2048,128]{1,0:T(8,128)(2,1)} %param.20) | copy-start | bytes 1572868
  47.4 1.9 %copy-start.2 = (bf16[1024,2048]{1,0:T(8,128)(2,1)}, bf16[1024,2048]{1,0:T(8,128)(2,1)S(1)}, u32[]{:S(2)}) copy-start(bf16[1024,2048]{1,0:T(8,128)(2,1)S(1)} %get-tuple-element.28.x_ref) | copy-start | bytes 12582916
  49.3 0.6 copy-start.3
  49.9 21.8 %copy-start.5 = (bf16[2048,256]{1,0:T(8,128)(2,1)S(1)}, bf16[2048,256]{1,0:T(8,128)(2,1)}, u32[]{:S(2)}) copy-start(bf16[2048,256]{1,0:T(8,128)(2,1)} %param.19) | copy-start | bytes 3145732
  74.3 3.6 %copy-start.8 = (f32[4]{0:T(128)S(1)}, f32[4]{0:T(128)}, u32[]{:S(2)}) copy-start(f32[4]{0:T(128)} %param.22) | copy-start | bytes 52
  86.2 2.2 %copy-start.1 = (bf16[1024,2048]{1,0:T(8,128)(2,1)S(1)}, bf16[1024,2048]{1,0:T(8,128)(2,1)}, u32[]{:S(2)}) copy-start(bf16[1024,2048]{1,0:T(8,128)(2,1)} %experts.1.moe_ref) | copy-start | bytes 12582916

commit v2 on v1

--- a/solution.py
+++ b/solution.py
@@ -90,9 +90,10 @@
         copy.start()
         started.append(copy)
 
-    for d in (3, 2, 1):
+    for d in (1, 2, 3):
         go(me, y, z_peer[d], zs_.at[d], zr_.at[d], own=True)
-    go(me, y, x_peer, xs_.at[0], xr_.at[0], own=True)
+        if d == 1:
+            go(me, y, x_peer, xs_.at[0], xr_.at[0], own=True)
     go(me, 1 - y, z_peer[1], zs_.at[0], zr_.at[0], own=True)
     go(me, 1 - y, x_peer, xs_.at[4], xr_.at[4], own=True)
 
@@ -146,12 +147,14 @@
         if d != 1:
             to_y(blk(d, x))
         to_core(blk(d, x), y)
-    arrived(blk(0, 1 - x), y, xr_.at[0], c_peer)
-    to_core(blk(0, 1 - x), y)
+        if d == 1:
+            arrived(blk(0, 1 - x), y, xr_.at[0], c_peer)
+            to_core(blk(0, 1 - x), y)
+        if d == 2:
+            arrived(blk(0, 1 - x), 1 - y, xr_.at[4], c_peer)
+            to_core(blk(0, 1 - x), 1 - y)
     arrived(blk(1, x), 1 - y, zr_.at[0], c_peer)
     to_core(blk(1, x), 1 - y)
-    arrived(blk(0, 1 - x), 1 - y, xr_.at[4], c_peer)
-    to_core(blk(0, 1 - x), 1 - y)
     for d in (1, 2, 3):
         arrived(blk(d, 1 - x), y, xr_.at[d], c_peer)
         to_y(blk(d, 1 - x))
@@ -510,36 +513,47 @@
         )
     keys_all = jnp.concatenate([keys_before, keys_local], axis=0)
     values_all = jnp.concatenate([values_before, values_local], axis=0)
-    layer_block = min(512, rows_first)
-    sink_scores = head_sink_logit.reshape(key_heads, head_group)[:, :, None, None]
-
-    def attend(index):
-        leading_row = index * layer_block
-        block_queries = query_rows.reshape(layer_block, key_heads, head_group, HEAD_SIZE)
-        scores = jnp.einsum(
-            "qhgd,khd->hgqk", block_queries, keys_all, preferred_element_type=jnp.float32
-        ) * HEAD_SIZE ** (-0.5)
-        query_pos = offset + leading_row + jnp.arange(layer_block, dtype=jnp.int32)
-        key_pos = (
-            offset
-            + leading_row
-            - BAND_LENGTH
-            + jnp.arange(layer_block + BAND_LENGTH, dtype=jnp.int32)
-        )
-        offsets = query_pos[:, None] - key_pos[None, :]
-        visible = (offsets >= 0) & (offsets < BAND_LENGTH) & (key_pos[None, :] >= 0)
-        scores = jnp.where(visible[None, None], scores, -jnp.inf)
-        peak = jnp.maximum(jnp.max(scores, axis=-1, keepdims=True), sink_scores)
-        expo = jnp.exp(scores - peak)
-        total = jnp.sum(expo, axis=-1, keepdims=True) + jnp.exp(sink_scores - peak)
-        weights = (expo / total).astype(jnp.bfloat16)
-        mixed = jnp.einsum(
-            "hgqk,khd->qhgd", weights, values_all, preferred_element_type=jnp.float32
-        )
-        return mixed.astype(jnp.bfloat16).reshape(layer_block, head_count * HEAD_SIZE)
-
-    attended = lax.map(attend, jnp.arange(rows_first // layer_block, dtype=jnp.int32)).reshape(
-        rows_first, head_count * HEAD_SIZE
+    band = BAND_LENGTH
+    bands = rows_first // band
+
+    def windows(padded):
+        return jnp.concatenate(
+            [
+                padded[:rows_first].reshape(bands, band, key_heads, HEAD_SIZE),
+                padded[band:].reshape(bands, band, key_heads, HEAD_SIZE),
+            ],
+            axis=1,
+        )
+
+    sink_scores = head_sink_logit.reshape(key_heads, head_group)[None, :, :, None, None]
+    scores = jnp.einsum(
+        "bqhgd,bkhd->bhgqk",
+        query_rows.reshape(bands, band, key_heads, head_group, HEAD_SIZE),
+        windows(keys_all),
+        preferred_element_type=jnp.float32,
+    ) * HEAD_SIZE ** (-0.5)
+    offsets = (
+        band
+        + jnp.arange(band, dtype=jnp.int32)[:, None]
+        - jnp.arange(2 * band, dtype=jnp.int32)[None, :]
+    )
+    key_pos = (
+        offset
+        + (jnp.arange(bands, dtype=jnp.int32)[:, None] - 1) * band
+        + jnp.arange(2 * band, dtype=jnp.int32)[None, :]
+    )
+    visible = ((offsets >= 0) & (offsets < band))[None] & (key_pos >= 0)[:, None, :]
+    scores = jnp.where(visible[:, None, None], scores, -jnp.inf)
+    peak = jnp.maximum(jnp.max(scores, axis=-1, keepdims=True), sink_scores)
+    expo = jnp.exp(scores - peak)
+    total = jnp.sum(expo, axis=-1, keepdims=True) + jnp.exp(sink_scores - peak)
+    weights = (expo / total).astype(jnp.bfloat16)
+    attended = (
+        jnp.einsum(
+            "bhgqk,bkhd->bqhgd", weights, windows(values_all), preferred_element_type=jnp.float32
+        )
+        .astype(jnp.bfloat16)
+        .reshape(rows_first, head_count * HEAD_SIZE)
     )
     if kernels:
         capacity = max(2, 2 * tokens_second.shape[0] * routes.shape[1] // (w_gate_exp.shape[0] * 8))

time: 129 us -> 117 us (0.907)
  matrix products: 14.2 us -> 6.33 us
  Pallas kernels: 96.4 us -> 93.1 us
  other arithmetic: 10.7 us -> 8 us
  local copies, waits for them, and re-layouts: 6 us -> 8.14 us
    dot_general x2, matrix products: 7.54 us -> 2.94 us  [the longest x1 1.55 us: local(): jnp.einsum('bhgqk,bkhd->bqhgd', weights, windows(values_all), preferred_e...]
    pallas_call x1, Pallas kernels: 36.6 us -> 32.5 us  [gather(): pl.pallas_call(functools.partial(gather_kernel, n_ep), out_shape=(jax.Sha...]
    reduce_sum x1, other arithmetic: 3.61 us -> 0.31 us  [local(): total = jnp.sum(expo, axis=-1, keepdims=True) + jnp.exp(sink_scores - peak)]
    dot_general x1, matrix products: 2.45 us -> 0.77 us  [local(): jnp.dot(norm_input, value_matrix, preferred_element_type=jnp.float32)]
    dot_general x1, matrix products: 2.53 us -> 0.95 us  [local(): jnp.dot(norm_input, w_query, preferred_element_type=jnp.float32)]
    slice x2, local copies, waits for them, and re-layouts: 0.12 us -> 1.47 us  [local(): values_before = before[:, split:].reshape(BAND_LENGTH, key_heads, HEAD_SIZE)]
    unnamed x20 -> x24, local copies, waits for them, and re-layouts: 5.46 us -> 4.33 us
where the time goes in v2:
time: 117 us
  Pallas kernels  93.1 us (80%)
  local copies, waits for them, and re-layouts  8.14 us (7%)
  other arithmetic  8 us (7%)
  matrix products  6.33 us (5%)
    pallas_call x1, Pallas kernels, reduce_both(): pl.pallas_call(reduce_kernel, out_shape=(jax.ShapeDtypeStruct((rows, widt...  39.2 us
    pallas_call x1, Pallas kernels, gather(): pl.pallas_call(functools.partial(gather_kernel, n_ep), out_shape=(jax.Sha...  32.5 us
    pallas_call x1, Pallas kernels, experts_of(): pl.pallas_call(functools.partial(ffn_kernel, cap), grid=(exp_dev,), out_s...  21.4 us
    unnamed x24, local copies, waits for them, and re-layouts  4.33 us
    reduce_sum x2, other arithmetic, rms_scale(): jnp.mean(wide * wide, axis=-1, keepdims=True) + norm_eps  3.45 us

profile of v2, /device:TPU:0, one launch (start us, length us, event | category | flops | bytes accessed | tf_op | source)
XLA Modules:
  0.0 116.5 jit_solution(12777972605247823127)
XLA Ops:
  0.7 1.4 %fusion.5 = f32[128]{0:T(128)S(1)} fusion(bf16[128,2048]{1,0:T(8,128)(2,1)} %param.24), kind=kLoop, calls=%fused_computation.15 | loop fusion | flops 786304 | bytes 524800 | tf_op jit(solution)/shard_map/reduce_sum | solution.py:26
  2.1 1.2 %fusion.7.x_ref = bf16[128,2048]{1,0:T(8,128)(2,1)S(1)} fusion(bf16[128,2048]{1,0:T(8,128)(2,1)} %param.24, f32[2048]{0:T(1024)} %param.25, f32[128]{0:T(128)S(1)} %add_rsqrt_fusion.1), kind=kLoop, calls=%fused_computation.17 | loop fusion | flops 1048576 | bytes 1057280 | tf_op jit(solution)/shard_map/convert_element_type | solution.py:27
  3.3 0.7 convert_element_type.43
  4.0 0.7 maximum_bitcast_fusion.4.meta_ref
  4.7 2.1 %fusion = f32[512]{0:T(512)S(1)} fusion(bf16[512,2048]{1,0:T(8,128)(2,1)} %param.17), kind=kLoop, calls=%fused_computation.2 | loop fusion | flops 3145216 | bytes 2099200 | tf_op jit(solution)/shard_map/reduce_sum | solution.py:26
  6.8 0.8 convolution_convert_fusion.2
  7.6 0.2 copy-done.8
  7.8 0.9 fusion.29
  8.8 0.3 multiply_cosine_fusion
  9.2 0.1 copy.27
  9.3 32.5 %gather_rows.1 = (bf16[1024,2048]{1,0:T(8,128)(2,1)S(1)}, f32[8,8,128]{2,1,0:T(8,128)S(1)}, bf16[128,256]{1,0:T(8,128)(2,1)S(1)}) custom-call(bf16[128,2048]{1,0:T(8,128)(2,1)S(1)} %fusion.7.x_ref, f32[8,128]{1,0:T(8,128)S(1)} %maximum_bitcast_fusion.4.meta_ref, bf16[128,256]{1,0:T(8,128)(2,1)S(1)} %pad_maximum_fusion.3.halo_ref), custom_call_target="tpu_custom_call" | custom-call | tf_op jit(solution)/shard_map/gather_rows/pallas_call | solution.py:192
  41.9 2.0 %copy-done.2 = bf16[1024,2048]{1,0:T(8,128)(2,1)} copy-done((bf16[1024,2048]{1,0:T(8,128)(2,1)}, bf16[1024,2048]{1,0:T(8,128)(2,1)S(1)}, u32[]{:S(2)}) %copy-start.2) | copy-done | bytes 4194328
  43.8 0.6 copy-done.3
  44.5 21.4 %experts.1.moe_ref = bf16[1024,2048]{1,0:T(8,128)(2,1)} custom-call(bf16[1024,2048]{1,0:T(8,128)(2,1)} %copy-done.2, f32[8,8,128]{2,1,0:T(8,128)} %copy-done.3, bf16[2,2048,512]{2,1,0:T(8,128)(2,1)} %wg_ref.1, bf16[2,2048,512]{2,1,0:T(8,128)(2,1)} %wu_ref.1, bf16[2,512,2048]{2,1,0:T(8,128)(2,1)} %wd_ref.1, bf16[2048,256]{1,0:T(8,128)(2,1)} %sg_ref.1, ...), custom_call_target="tpu_custom_call" | custom-call | tf_op jit(solution)/shard_map/experts/pallas_call | solution.py:277
  65.9 1.0 fusion.26
  67.1 0.7 copy_bitcast_fusion.2
  67.7 0.6 fusion.31
  68.3 0.1 copy.33
  68.6 0.2 broadcast_and_fusion
  68.8 1.4 %fusion.32 = (f32[4,2,2,128]{3,2,1,0:T(2,128)S(1)}, f32[4,2,2,128,256]{3,4,2,1,0:T(8,128)S(1)}) fusion(bf16[4,128,2,2,32]{1,4,3,2,0:T(8,128)(2,1)S(1)} %copy.38, bf16[4,128,2,2,32]{1,4,3,2,0:T(8,128)(2,1)S(1)} %copy.37, bf16[4,128,2,32]{1,3,2,0:T(8,128)(2,1)} %get-tuple-element.22, bf16[4,128,2,32]{1,3,2,0:T(8,128)(2,1)} %get-tuple-element.23, ...), kind=kOutput, calls=%fused_computation.68 | convolution fusion | flops 69990400 | bytes 2760704 | tf_op jit(solution)/shard_map/bqhgd,bkhd->bhgqk/dot_general | solution.py:529
  70.4 0.3 fusion.3
  70.7 0.7 exponential_add_fusion
  71.4 0.1 reshape.204
  71.5 0.8 copy.32
  72.3 0.1 copy.29
  72.4 0.9 copy.28
  73.4 1.5 %fusion.4 = bf16[4,128,2,2,64]{1,4,3,2,0:T(8,128)(2,1)S(1)} fusion(f32[4,2,2,128,256]{3,4,2,1,0:T(8,128)S(1)} %get-tuple-element.21, f32[4,2,2,128]{3,2,1,0:T(2,128)} %exponential_add_fusion, f32[4,2,2,128]{3,2,1,0:T(2,128)S(1)} %broadcast_maximum_fusion, bf16[4,128,2,64]{1,3,2,0:T(8,128)(2,1)} %copy.32, bf16[4,128,2,64]{1,3,2,0:T(8,128)(2,1)S(1)} %copy_bitcast_fusion.1), kind=kOutput, calls=%fused_computation.13 | convolution fusion | flops 69337088 | bytes 2637824 | tf_op jit(solution)/shard_map/bhgqk,bkhd->bqhgd/dot_general | solution.py:552
  74.9 0.2 copy.40
  75.1 0.7 convolution_convert_fusion.mix_ref
  75.9 39.2 %reduce_both.1 = (bf16[128,512]{1,0:T(8,128)(2,1)S(1)}, bf16[128,2048]{1,0:T(8,128)(2,1)S(1)}) custom-call(bf16[1024,2048]{1,0:T(8,128)(2,1)S(1)} %copy-done.1, bf16[512,2048]{1,0:T(8,128)(2,1)S(1)} %convolution_convert_fusion.mix_ref), custom_call_target="tpu_custom_call" | custom-call | tf_op jit(solution)/shard_map/reduce_both/pallas_call | solution.py:420
  115.1 0.8 copy.62
  115.8 0.7 copy.63
  (40 shorter events, 0.7 us)
Async XLA Ops:
  0.6 74.5 %copy-start = (bf16[256,2048]{1,0:T(8,128)(2,1)S(1)}, bf16[256,2048]{1,0:T(8,128)(2,1)}, u32[]{:S(2)}) copy-start(bf16[256,2048]{1,0:T(8,128)(2,1)} %param.23) | copy-start | bytes 3145732
  0.6 6.1 %copy-start.7 = (bf16[2048,128]{1,0:T(8,128)(2,1)S(1)}, bf16[2048,128]{1,0:T(8,128)(2,1)}, u32[]{:S(2)}) copy-start(bf16[2048,128]{1,0:T(8,128)(2,1)} %param.21) | copy-start | bytes 1572868
  0.7 6.1 %copy-start.4 = (bf16[512,2048]{1,0:T(8,128)(2,1)S(1)}, bf16[512,2048]{1,0:T(8,128)(2,1)}, u32[]{:S(2)}) copy-start(bf16[512,2048]{1,0:T(8,128)(2,1)} %param.17) | copy-start | bytes 6291460
  0.7 6.1 %copy-start.9 = (f32[2048]{0:T(1024)S(1)}, f32[2048]{0:T(1024)}, u32[]{:S(2)}) copy-start(f32[2048]{0:T(1024)} %param.18) | copy-start | bytes 24580
  6.8 1.0 copy-start.8
  41.8 2.0 %copy-start.2 = (bf16[1024,2048]{1,0:T(8,128)(2,1)}, bf16[1024,2048]{1,0:T(8,128)(2,1)S(1)}, u32[]{:S(2)}) copy-start(bf16[1024,2048]{1,0:T(8,128)(2,1)S(1)} %get-tuple-element.7.x_ref) | copy-start | bytes 12582916
  43.8 0.6 copy-start.3
  44.4 21.4 %copy-start.5 = (bf16[512,2048]{1,0:T(8,128)(2,1)S(1)}, bf16[512,2048]{1,0:T(8,128)(2,1)}, u32[]{:S(2)}) copy-start(bf16[512,2048]{1,0:T(8,128)(2,1)} %param.17) | copy-start | bytes 6291460
  44.4 21.4 %copy-start.6 = (bf16[2048,256]{1,0:T(8,128)(2,1)S(1)}, bf16[2048,256]{1,0:T(8,128)(2,1)}, u32[]{:S(2)}) copy-start(bf16[2048,256]{1,0:T(8,128)(2,1)} %param.19) | copy-start | bytes 3145732
  67.0 3.2 %copy-start.10 = (f32[4]{0:T(128)S(1)}, f32[4]{0:T(128)}, u32[]{:S(2)}) copy-start(f32[4]{0:T(128)} %param.22) | copy-start | bytes 52
  73.3 2.5 %copy-start.1 = (bf16[1024,2048]{1,0:T(8,128)(2,1)S(1)}, bf16[1024,2048]{1,0:T(8,128)(2,1)}, u32[]{:S(2)}) copy-start(bf16[1024,2048]{1,0:T(8,128)(2,1)} %experts.1.moe_ref) | copy-start | bytes 12582916
